TPU v7x, 32 devices: a whole 2x2x4 slice. The times are simulated.
32 devices in a mesh: sp: 8 (over z, y), tp: 4 (over x, core).
Axes of the slice: x: 2, y: 2, z: 4, core: 2. Of those that a mesh axis runs over, the one named last changes fastest.
Arguments:
- query_a: bfloat16 [1536, 2048], P('sp', 'tp'), may hold values from -7.5 to 7.5
- key_a: bfloat16 [1536, 1024], P('sp', 'tp'), may hold values from -7.5 to 7.5
- value_a: bfloat16 [1536, 1024], P('sp', 'tp'), may hold values from -6 to 6
- query_b: bfloat16 [1536, 2048], P('sp', 'tp'), may hold values from -7.5 to 7.5
- key_b: bfloat16 [1536, 512], P('sp', 'tp'), may hold values from -7.5 to 7.5
- value_b: bfloat16 [1536, 512], P('sp', 'tp'), may hold values from -6 to 6
- gain_a: float32 [2, 128], replicated, may hold values from 1 to 6.5
- gain_b: float32 [2, 64], replicated, may hold values from 1 to 8.5
- out_a: bfloat16 [2048, 4096], P('tp'), may hold values from -0.5 to 0.5
- out_b: bfloat16 [2048, 4096], P('tp'), may hold values from -0.5 to 0.5
- residual: bfloat16 [1536, 4096], P('sp'), may hold values from -6 to 6
- norm_gain: float32 [4096], replicated, may hold values from 0.1 to 1.9
- gate_weight: bfloat16 [4096, 6144], P('sp', 'tp'), may hold values from -0.09375 to 0.09375
- up_weight: bfloat16 [4096, 6144], P('sp', 'tp'), may hold values from -0.09375 to 0.09375
- down_weight: bfloat16 [6144, 4096], P('tp', 'sp'), may hold values from -0.3125 to 0.3125
Outputs:
- output: bfloat16 [1536, 4096], P(('sp', 'tp'))
All inputs are finite; a program needn't handle non-finite values.
Results may differ from a plain program's by a relative error of at most 0.017.
The roundings to bfloat16 on the way count: a program that leaves them out, or rounds other values in their place, can miss the bound.
Values may be sent and summed in bfloat16 or wider, within the bound.
A program may use at most 128 MiB of HBM per device.

v0:
```python
import jax
import jax.numpy as jnp
from jax import lax
from jax.sharding import PartitionSpec as P

HEAD_A = 128
HEAD_B = 64
GRID_W = 64
epsilon = 1e-06
theta_base = 10000.0


def rotate(inputs, num_heads, head_size, first_pos, gain):
    tok_rows = inputs.shape[0]
    vectors = inputs.astype(jnp.float32).reshape(tok_rows, num_heads, head_size)
    vectors = (
        vectors * lax.rsqrt(jnp.mean(vectors * vectors, axis=-1, keepdims=True) + epsilon) * gain
    )
    position = first_pos + jnp.arange(tok_rows, dtype=jnp.int32)
    grid_row = (position // GRID_W).astype(jnp.float32)
    grid_col = (position % GRID_W).astype(jnp.float32)
    quarter = head_size // 4
    inv_freq = theta_base ** (-4.0 * jnp.arange(quarter, dtype=jnp.float32) / head_size)
    angle_row = grid_row[:, None] * inv_freq[None, :]
    angle_col = grid_col[:, None] * inv_freq[None, :]
    angles = jnp.concatenate([angle_row, angle_row, angle_col, angle_col], axis=-1)
    quarters = vectors.reshape(tok_rows, num_heads, 4, quarter)
    rotated = jnp.stack(
        [-quarters[:, :, 1], quarters[:, :, 0], -quarters[:, :, 3], quarters[:, :, 2]], axis=2
    )
    rotated = rotated.reshape(tok_rows, num_heads, head_size)
    result = vectors * jnp.cos(angles)[:, None, :] + rotated * jnp.sin(angles)[:, None, :]
    return result.reshape(tok_rows, num_heads * head_size).astype(jnp.bfloat16)


def start_state(kv_heads, groups, tok_rows, head_size):
    return (
        jnp.full((kv_heads, groups, tok_rows), -1e30, jnp.float32),
        jnp.zeros((kv_heads, groups, tok_rows), jnp.float32),
        jnp.zeros((kv_heads, groups, tok_rows, head_size), jnp.float32),
    )


def attend(state, queries, key_rows, values, head_size):
    run_max, run_sum, run_acc = state
    kv_heads = key_rows.shape[1] // head_size
    groups = run_max.shape[1]
    q_heads = queries.reshape(queries.shape[0], kv_heads, groups, head_size)
    k_heads = key_rows.reshape(key_rows.shape[0], kv_heads, head_size)
    v_heads = values.reshape(values.shape[0], kv_heads, head_size)
    scores = jnp.einsum(
        "tkgd,pkd->kgtp", q_heads, k_heads, preferred_element_type=jnp.float32
    ) * head_size ** (-0.5)
    new_max = jnp.maximum(run_max, jnp.max(scores, axis=-1))
    exp_scores = jnp.exp(scores - new_max[..., None])
    new_sum = jnp.sum(exp_scores, axis=-1)
    new_acc = jnp.einsum(
        "kgtp,pkd->kgtd",
        exp_scores.astype(jnp.bfloat16),
        v_heads,
        preferred_element_type=jnp.float32,
    )
    return (new_max, new_sum, new_acc)


def finish(state, num_cols):
    blended = state[2] / state[1][..., None]
    return blended.transpose(2, 0, 1, 3).reshape(blended.shape[2], num_cols).astype(jnp.bfloat16)


def normalize(mixed_rows, gain):
    scale = lax.rsqrt(jnp.mean(mixed_rows * mixed_rows, axis=-1, keepdims=True) + epsilon)
    return (mixed_rows * scale * gain).astype(jnp.bfloat16)


def on_device(
    query_a,
    key_a,
    value_a,
    query_b,
    key_b,
    value_b,
    gain_a,
    gain_b,
    out_a,
    out_b,
    residual,
    norm_gain,
    gate_weight,
    up_weight,
    down_weight,
):
    tok_rows = query_a.shape[0]
    first_pos = lax.axis_index("sp") * tok_rows
    heads_a = query_a.shape[1] // HEAD_A
    heads_b = query_b.shape[1] // HEAD_B
    kv_heads_a = key_a.shape[1] // HEAD_A
    kv_heads_b = key_b.shape[1] // HEAD_B
    kv_width_b = kv_heads_b * HEAD_B
    turned_qa = rotate(query_a, heads_a, HEAD_A, first_pos, gain_a[0])
    turned_ka = rotate(key_a, kv_heads_a, HEAD_A, first_pos, gain_a[1])
    turned_qb = rotate(query_b, heads_b, HEAD_B, first_pos, gain_b[0])
    turned_kb = rotate(key_b, kv_heads_b, HEAD_B, first_pos, gain_b[1])
    pair_b = jnp.concatenate([turned_kb, value_b], axis=1)
    initial = (
        start_state(kv_heads_a, heads_a // kv_heads_a, tok_rows, HEAD_A),
        start_state(kv_heads_b, heads_b // kv_heads_b, tok_rows, HEAD_B),
    )
    pieces = (
        lax.all_gather(turned_ka, "sp", axis=0, tiled=True),
        lax.all_gather(value_a, "sp", axis=0, tiled=True),
        lax.all_gather(pair_b, "sp", axis=0, tiled=True),
    )
    state_a = attend(initial[0], turned_qa, pieces[0], pieces[1], HEAD_A)
    state_b = attend(
        initial[1], turned_qb, pieces[2][:, :kv_width_b], pieces[2][:, kv_width_b:], HEAD_B
    )
    attn_a = finish(state_a, query_a.shape[1])
    attn_b = finish(state_b, query_b.shape[1])
    own_rows = tok_rows // lax.axis_size("tp")
    own_start = lax.axis_index("tp") * own_rows
    head_sum = lax.psum(
        (
            jnp.dot(attn_a, out_a, preferred_element_type=jnp.float32)
            + jnp.dot(attn_b, out_b, preferred_element_type=jnp.float32)
        ).astype(jnp.bfloat16),
        "tp",
    ).astype(jnp.float32)
    whole_mixed = residual.astype(jnp.float32) + head_sum
    normed = normalize(whole_mixed, norm_gain)
    mixed_rows = lax.dynamic_slice_in_dim(whole_mixed, own_start, own_rows, 0)
    pieces = (
        lax.all_gather(gate_weight, "sp", axis=0, tiled=True),
        lax.all_gather(up_weight, "sp", axis=0, tiled=True),
    )
    gate_act = jnp.dot(normed, pieces[0], preferred_element_type=jnp.float32)
    up_act = jnp.dot(normed, pieces[1], preferred_element_type=jnp.float32)
    hidden = (jax.nn.silu(gate_act) * up_act).astype(jnp.bfloat16)
    down_all = jnp.dot(
        hidden,
        lax.all_gather(down_weight, "sp", axis=1, tiled=True),
        preferred_element_type=jnp.float32,
    )
    branch_sum = lax.psum_scatter(
        down_all.astype(jnp.bfloat16), "tp", scatter_dimension=0, tiled=True
    ).astype(jnp.float32)
    return (mixed_rows + 0.5 * branch_sum).astype(jnp.bfloat16)


def solution(mesh):
    return jax.shard_map(
        on_device,
        mesh=mesh,
        in_specs=(
            P("sp", "tp"),
            P("sp", "tp"),
            P("sp", "tp"),
            P("sp", "tp"),
            P("sp", "tp"),
            P("sp", "tp"),
            P(),
            P(),
            P("tp", None),
            P("tp", None),
            P("sp", None),
            P(),
            P("sp", "tp"),
            P("sp", "tp"),
            P("tp", "sp"),
        ),
        out_specs=P(("sp", "tp"), None),
        check_vma=False,
    )
```

profile of v0, /device:TPU:0, one launch (start us, length us, event | category | flops | bytes accessed | tf_op | source)
XLA Modules:
  0.0 724.6 jit_solution(1680261890716808169)
XLA Ops:
  7.4 1.0 copy.39
  8.4 0.8 slice_reduce_fusion
  9.2 0.1 mul.497
  9.3 0.1 multiply_multiply_fusion.3
  9.4 0.1 mul.484
  9.5 0.9 copy.40
  10.4 0.1 broadcast_multiply_fusion.3
  10.5 0.1 fusion.48
  10.6 0.1 fusion.43
  10.7 0.1 copy.41
  10.9 33.9 %all_gather.20 = bf16[1536,256]{1,0:T(8,128)(2,1)S(1)} all-gather(bf16[192,256]{1,0:T(8,128)(2,1)S(1)} %copy.41), channel_id=1, replica_groups=mesh['sp'=8,'tp'=4] {'sp'}, dimensions={0}, use_global_device_ids=true | all-gather | bytes 884736 | tf_op jit(solution)/shard_map/all_gather | solution.py:112
  44.7 0.1 fusion.56
  44.8 0.2 copy.42
  45.0 0.1 copy.43
  45.1 0.1 bitcast_reduce_fusion.2
  45.2 0.1 mul.518
  45.3 0.1 multiply_multiply_fusion
  45.5 0.1 mul.510
  45.6 0.2 fusion.34
  45.8 5.1 bitcast_reduce_fusion
  50.9 0.2 copy.44
  51.1 0.1 copy.33
  51.2 0.1 bitcast_reduce_fusion.3
  51.3 0.1 mul.468
  51.4 0.1 multiply_multiply_fusion.1
  51.6 0.1 broadcast_multiply_fusion.1
  51.7 0.1 copy-done.5
  51.8 0.1 copy.30
  51.9 0.1 mul.447
  52.0 0.1 multiply_multiply_fusion.2
  52.1 0.2 fusion.46
  52.4 0.1 fusion.40
  52.5 0.1 copy.31
  52.6 32.3 %all_gather.18 = bf16[1536,256]{1,0:T(8,128)(2,1)S(1)} all-gather(bf16[192,256]{1,0:T(8,128)(2,1)S(1)} %copy.31), channel_id=1, replica_groups=mesh['sp'=8,'tp'=4] {'sp'}, dimensions={0}, use_global_device_ids=true | all-gather | bytes 884736 | tf_op jit(solution)/shard_map/all_gather | solution.py:110
  84.9 0.3 copy.32
  85.3 0.2 fusion.37
  85.5 3.1 bitcast_reduce_fusion.1
  88.5 32.2 %all_gather.19 = bf16[1536,256]{1,0:T(8,128)(2,1)S(1)} all-gather(bf16[192,256]{1,0:T(8,128)(2,1)S(1)} %copy-done.6), channel_id=1, replica_groups=mesh['sp'=8,'tp'=4] {'sp'}, dimensions={0}, use_global_device_ids=true | all-gather | bytes 884736 | tf_op jit(solution)/shard_map/all_gather | solution.py:111
  120.7 0.3 copy.36
  121.0 3.4 fusion.7
  124.4 0.3 copy-done
  124.8 1.0 fusion.23
  125.8 0.2 copy.38
  126.0 0.1 convert_element_type.95
  126.1 5.4 fusion.1
  131.5 5.7 fusion.29
  137.2 1.0 fusion.57
  138.2 1.2 copy-done.2
  139.4 2.2 fusion.3
  141.6 0.0 all-gather.4.cloned.1.call-start
  141.7 0.5 all-gather.4.cloned.1.call-update
  142.2 0.0 all-gather.6.cloned.1.call-start
  142.2 0.5 all-gather.6.cloned.1.call-update
  142.8 0.5 all-gather.8.cloned.1.call-update
  143.4 0.3 reduce-scatter.2.cloned.1.call-start
  143.6 41.4 %all-reduce.2.cloned.1.call-done = bf16[192,4096]{1,0:T(8,128)(2,1)} async-done(((bf16[192,4096]{1,0:T(8,128)(2,1)}), bf16[192,4096]{1,0:T(8,128)(2,1)}) %all-reduce.2.cloned.1.call-update) | async-done | bytes 1572880 | tf_op jit(solution)/shard_map/psum | solution.py:122
  185.1 2.5 convert_add_fusion
  187.6 133.1 %all-gather.4.cloned.1.call-done = bf16[4096,1536]{1,0:T(8,128)(2,1)} async-done(((bf16[512,1536]{1,0:T(8,128)(2,1)}), bf16[4096,1536]{1,0:T(8,128)(2,1)}) %all-gather.4.cloned.1.call-update) | async-done | bytes 12582928 | tf_op jit(solution)/shard_map/all_gather | solution.py:133
  320.7 9.2 %fusion.55 = f32[192,1536]{1,0:T(8,128)} fusion(bf16[4096,1536]{1,0:T(8,128)(2,1)} %all-gather.4.cloned.1.call-done, f32[4096]{0:T(1024)S(1)} %copy-done.8, f32[192]{0:T(256)S(1)} %add_rsqrt_fusion.4, bf16[192,4096]{1,0:T(8,128)(2,1)} %all-reduce.2.cloned.1.call-done, bf16[192,4096]{1,0:T(8,128)(2,1)} %param.25), kind=kOutput, calls=%fused_computation.121 | convolution fusion | flops 2420637696 | bytes 16925440 | tf_op jit(solution)/shard_map/dot_general | solution.py:136
  329.9 167.0 %all-gather.6.cloned.1.call-done = bf16[4096,1536]{1,0:T(8,128)(2,1)} async-done(((bf16[512,1536]{1,0:T(8,128)(2,1)}), bf16[4096,1536]{1,0:T(8,128)(2,1)}) %all-gather.6.cloned.1.call-update) | async-done | bytes 12582928 | tf_op jit(solution)/shard_map/all_gather | solution.py:134
  496.9 176.0 %all-gather.8.cloned.1.call-done = bf16[1536,4096]{1,0:T(8,128)(2,1)} async-done(((bf16[1536,512]{1,0:T(8,128)(2,1)}), bf16[1536,4096]{1,0:T(8,128)(2,1)}) %all-gather.8.cloned.1.call-update) | async-done | bytes 12582928 | tf_op jit(solution)/shard_map/all_gather | solution.py:141
  672.9 15.9 %convolution_convert_fusion = bf16[192,4096]{1,0:T(8,128)(2,1)} fusion(bf16[1536,4096]{1,0:T(8,128)(2,1)} %all-gather.8.cloned.1.call-done, bf16[4096,1536]{1,0:T(8,128)(2,1)} %all-gather.6.cloned.1.call-done, f32[192,1536]{1,0:T(8,128)} %fusion.55, f32[4096]{0:T(1024)S(1)} %copy-done.8, f32[192]{0:T(256)S(1)} %add_rsqrt_fusion.4, ...), kind=kOutput, calls=%fused_computation.7 | convolution fusion | flops 4839112704 | bytes 31081216 | tf_op jit(solution)/shard_map/dot_general | solution.py:139
  688.8 26.4 %reduce-scatter.2.cloned.1.call-done = bf16[48,4096]{1,0:T(8,128)(2,1)} async-done(((bf16[192,4096]{1,0:T(8,128)(2,1)}), bf16[48,4096]{1,0:T(8,128)(2,1)}) %reduce-scatter.2.cloned.1.call-update) | async-done | bytes 393232 | tf_op jit(solution)/shard_map/reduce_scatter | solution.py:144
  715.2 1.8 add_convert_fusion
  (45 shorter events, 0.6 us)
Async XLA Ops:
  7.4 37.6 %copy-start.3 = (bf16[192,512]{1,0:T(8,128)(2,1)S(1)}, bf16[192,512]{1,0:T(8,128)(2,1)}, u32[]{:S(2)}) copy-start(bf16[192,512]{1,0:T(8,128)(2,1)} %param.18) | copy-start | bytes 589828
  7.4 177.7 %all-reduce.2.cloned.1.call-start = ((), (), s32[]{:S(2)}) async-start(), calls=%async_computation.1 | async-start | bytes 3145728 | tf_op jit(solution)/shard_map/psum | solution.py:122
  45.8 5.3 copy-start.4
  45.8 5.5 copy-start.7
  50.9 0.9 copy-start.5
  85.4 3.1 copy-start.6
  121.0 3.8 copy-start
  131.4 5.7 copy-start.1
  137.2 2.2 copy-start.2
  141.6 179.1 %all-gather.4.cloned.1.call-start = ((), (), s32[]{:S(2)}) async-start(), calls=%async_computation.2 | async-start | bytes 14155776 | tf_op jit(solution)/shard_map/all_gather | solution.py:133
  142.2 354.7 %all-gather.6.cloned.1.call-start = ((), (), s32[]{:S(2)}) async-start(), calls=%async_computation.3 | async-start | bytes 14155776 | tf_op jit(solution)/shard_map/all_gather | solution.py:134
  142.8 530.2 %all-gather.8.cloned.1.call-start = ((), (), s32[]{:S(2)}) async-start(), calls=%async_computation.4 | async-start | bytes 14155776 | tf_op jit(solution)/shard_map/all_gather | solution.py:141
  143.4 177.3 %copy-start.8 = (f32[4096]{0:T(1024)S(1)}, f32[4096]{0:T(1024)}, u32[]{:S(2)}) copy-start(f32[4096]{0:T(1024)} %param.26) | copy-start | bytes 49156
  143.4 571.8 %reduce-scatter.2.cloned.1.call-start = ((), (), s32[]{:S(2)}) async-start(), calls=%async_computation.5 | async-start | bytes 1966080 | tf_op jit(solution)/shard_map/reduce_scatter | solution.py:144
Sparse Core Ops, SparseCore 0:
  141.7 43.2 all-reduce.1
  688.9 26.2 reduce-scatter.1
Sparse Core Ops, SparseCore 1:
  144.3 176.3 all-gather.3
  322.8 174.1 all-gather.5
  498.8 174.1 all-gather.7
where the time goes:
time: 725 us
  waiting for transfers between devices  546 us (75%)
  blocking collectives  98.4 us (14%)
  matrix products  43.1 us (6%)
  between operations  15.4 us (2%)
  other arithmetic  15.1 us (2%)
    all_gather x1, waiting for transfers between devices, on_device(): lax.all_gather(down_weight, 'sp', axis=1, tiled=True)  176 us
    all_gather x1, waiting for transfers between devices, on_device(): lax.all_gather(up_weight, 'sp', axis=0, tiled=True)  167 us
    all_gather x1, waiting for transfers between devices, on_device(): lax.all_gather(gate_weight, 'sp', axis=0, tiled=True)  133 us
    psum x1, waiting for transfers between devices, on_device(): lax.psum((jnp.dot(attn_a, out_a, preferred_element_type=jnp.float32) + jn...  41.4 us
    all_gather x1, blocking collectives, on_device(): lax.all_gather(pair_b, 'sp', axis=0, tiled=True)  33.9 us
    all_gather x1, blocking collectives, on_device(): lax.all_gather(turned_ka, 'sp', axis=0, tiled=True)  32.3 us
    all_gather x1, blocking collectives, on_device(): lax.all_gather(value_a, 'sp', axis=0, tiled=True)  32.2 us
    reduce_scatter x1, waiting for transfers between devices, on_device(): lax.psum_scatter(down_all.astype(jnp.bfloat16), 'tp', scatter_dimension=0...  26.4 us
  transfers between devices with their start and end apart: 5, of which 5 were waited for; matrix products, arithmetic and copies ran while one was open for 2% of the time, Pallas kernels for 0%

commit v1 on v0

--- a/solution.py
+++ b/solution.py
@@ -8,6 +8,12 @@
 GRID_W = 64
 epsilon = 1e-06
 theta_base = 10000.0
+
+
+def summed_here(x, mesh_axis):
+    parts = lax.all_gather(x, mesh_axis, axis=0, tiled=False)
+    acc = parts.sum(axis=0)
+    return acc
 
 
 def rotate(inputs, num_heads, head_size, first_pos, gain):
@@ -119,7 +125,7 @@
     attn_b = finish(state_b, query_b.shape[1])
     own_rows = tok_rows // lax.axis_size("tp")
     own_start = lax.axis_index("tp") * own_rows
-    head_sum = lax.psum(
+    head_sum = summed_here(
         (
             jnp.dot(attn_a, out_a, preferred_element_type=jnp.float32)
             + jnp.dot(attn_b, out_b, preferred_element_type=jnp.float32)

time: 725 us -> 769 us (1.061)
  waiting for transfers between devices: 546 us -> 589 us
    all_gather x0 -> x1, waiting for transfers between devices: none -> 44.5 us  [summed_here(): parts = lax.all_gather(x, mesh_axis, axis=0, tiled=False)]
    psum x1 -> x0, waiting for transfers between devices: 41.4 us -> none  [on_device(): lax.psum((jnp.dot(attn_a, out_a, preferred_element_type=jnp.float32) + jn...]
    all_gather x1, waiting for transfers between devices: 133 us -> 172 us  [on_device(): lax.all_gather(gate_weight, 'sp', axis=0, tiled=True)]
    all_gather x1, waiting for transfers between devices: 167 us -> 176 us  [on_device(): lax.all_gather(up_weight, 'sp', axis=0, tiled=True)]
    all_gather x1, waiting for transfers between devices: 176 us -> 168 us  [on_device(): lax.all_gather(down_weight, 'sp', axis=1, tiled=True)]
where the time goes in v1:
time: 769 us
  waiting for transfers between devices  589 us (77%)
  blocking collectives  98.5 us (13%)
  matrix products  41.2 us (5%)
  other arithmetic  19.3 us (3%)
  between operations  13.6 us (2%)
    all_gather x1, waiting for transfers between devices, on_device(): lax.all_gather(up_weight, 'sp', axis=0, tiled=True)  176 us
    all_gather x1, waiting for transfers between devices, on_device(): lax.all_gather(gate_weight, 'sp', axis=0, tiled=True)  172 us
    all_gather x1, waiting for transfers between devices, on_device(): lax.all_gather(down_weight, 'sp', axis=1, tiled=True)  168 us
    all_gather x1, waiting for transfers between devices, summed_here(): parts = lax.all_gather(x, mesh_axis, axis=0, tiled=False)  44.5 us
    all_gather x1, blocking collectives, on_device(): lax.all_gather(pair_b, 'sp', axis=0, tiled=True)  33.9 us
    all_gather x1, blocking collectives, on_device(): lax.all_gather(turned_ka, 'sp', axis=0, tiled=True)  32.3 us
    all_gather x1, blocking collectives, on_device(): lax.all_gather(value_a, 'sp', axis=0, tiled=True)  32.3 us
    reduce_scatter x1, waiting for transfers between devices, on_device(): lax.psum_scatter(down_all.astype(jnp.bfloat16), 'tp', scatter_dimension=0...  26.4 us
  transfers between devices with their start and end apart: 5, of which 5 were waited for; matrix products, arithmetic and copies ran while one was open for 2% of the time, Pallas kernels for 0%

profile of v1, /device:TPU:0, one launch (start us, length us, event | category | flops | bytes accessed | tf_op | source)
XLA Modules:
  0.0 768.7 jit_solution(569485754671065084)
XLA Ops:
  6.6 1.0 copy.39
  7.6 0.8 slice_reduce_fusion
  8.3 0.1 mul.497
  8.4 0.1 multiply_multiply_fusion.3
  8.6 0.1 mul.484
  8.7 0.9 copy.40
  9.6 0.1 broadcast_multiply_fusion.3
  9.6 0.1 fusion.48
  9.8 0.1 fusion.43
  9.9 0.1 copy.41
  10.0 33.9 %all_gather.26 = bf16[1536,256]{1,0:T(8,128)(2,1)S(1)} all-gather(bf16[192,256]{1,0:T(8,128)(2,1)S(1)} %copy.41), channel_id=1, replica_groups=mesh['sp'=8,'tp'=4] {'sp'}, dimensions={0}, use_global_device_ids=true | all-gather | bytes 884736 | tf_op jit(solution)/shard_map/all_gather | solution.py:118
  43.9 0.1 fusion.56
  44.0 0.2 copy.42
  44.2 0.1 copy.43
  44.3 0.1 bitcast_reduce_fusion.2
  44.4 0.1 mul.518
  44.5 0.1 multiply_multiply_fusion
  44.6 0.1 mul.510
  44.8 0.2 fusion.34
  45.0 5.1 bitcast_reduce_fusion
  50.0 0.2 copy.44
  50.2 0.1 copy.33
  50.4 0.1 bitcast_reduce_fusion.3
  50.5 0.1 mul.468
  50.6 0.1 multiply_multiply_fusion.1
  50.7 0.1 broadcast_multiply_fusion.1
  50.8 0.1 copy-done.6
  50.9 0.1 copy.30
  51.1 0.1 mul.447
  51.2 0.1 multiply_multiply_fusion.2
  51.3 0.2 fusion.46
  51.6 0.1 fusion.40
  51.7 0.1 copy.31
  51.8 32.3 %all_gather.24 = bf16[1536,256]{1,0:T(8,128)(2,1)S(1)} all-gather(bf16[192,256]{1,0:T(8,128)(2,1)S(1)} %copy.31), channel_id=1, replica_groups=mesh['sp'=8,'tp'=4] {'sp'}, dimensions={0}, use_global_device_ids=true | all-gather | bytes 884736 | tf_op jit(solution)/shard_map/all_gather | solution.py:116
  84.2 0.3 copy.32
  84.5 0.2 fusion.37
  84.7 3.1 bitcast_reduce_fusion.1
  87.7 32.3 %all_gather.25 = bf16[1536,256]{1,0:T(8,128)(2,1)S(1)} all-gather(bf16[192,256]{1,0:T(8,128)(2,1)S(1)} %copy-done.7), channel_id=1, replica_groups=mesh['sp'=8,'tp'=4] {'sp'}, dimensions={0}, use_global_device_ids=true | all-gather | bytes 884736 | tf_op jit(solution)/shard_map/all_gather | solution.py:117
  120.0 0.3 copy.36
  120.3 3.4 fusion.7
  123.7 0.3 copy-done
  124.1 1.0 fusion.23
  125.0 0.2 copy.38
  125.3 0.1 convert_element_type.97
  125.3 5.4 fusion.1
  130.7 5.7 fusion.29
  136.5 1.0 fusion.57
  137.5 1.2 copy-done.2
  138.7 2.2 fusion.3
  140.9 0.0 all-gather.6.cloned.1.call-start
  140.9 0.7 all-gather.6.cloned.1.call-update
  141.7 0.7 all-gather.10.cloned.1.call-update
  142.4 0.5 all-gather.8.cloned.1.call-update
  142.9 0.3 reduce-scatter.2.cloned.1.call-start
  143.2 44.5 %all-gather.12.cloned.1.call-done = bf16[768,4096]{1,0:T(8,128)(2,1)} async-done(((bf16[192,4096]{1,0:T(8,128)(2,1)}), bf16[768,4096]{1,0:T(8,128)(2,1)}) %all-gather.12.cloned.1.call-update) | async-done | bytes 6291472 | tf_op jit(solution)/shard_map/all_gather | solution.py:14
  187.7 4.2 reduce_sum.81
  192.0 2.1 convert_add_fusion
  194.1 171.9 %all-gather.6.cloned.1.call-done = bf16[4096,1536]{1,0:T(8,128)(2,1)} async-done(((bf16[512,1536]{1,0:T(8,128)(2,1)}), bf16[4096,1536]{1,0:T(8,128)(2,1)}) %all-gather.6.cloned.1.call-update) | async-done | bytes 12582928 | tf_op jit(solution)/shard_map/all_gather | solution.py:139
  366.0 8.3 %fusion.55 = f32[192,1536]{1,0:T(8,128)} fusion(bf16[4096,1536]{1,0:T(8,128)(2,1)} %all-gather.6.cloned.1.call-done, f32[4096]{0:T(1024)S(1)} %copy-done.9, f32[192]{0:T(256)S(1)} %add_rsqrt_fusion.4, bf16[192,4096]{1,0:T(8,128)(2,1)S(1)} %reduce_sum.81, bf16[192,4096]{1,0:T(8,128)(2,1)S(1)} %copy-done.3), kind=kOutput, calls=%fused_computation.121 | convolution fusion | flops 2420637696 | bytes 16925440 | tf_op jit(solution)/shard_map/dot_general | solution.py:142
  374.3 168.1 %all-gather.10.cloned.1.call-done = bf16[1536,4096]{1,0:T(8,128)(2,1)} async-done(((bf16[1536,512]{1,0:T(8,128)(2,1)}), bf16[1536,4096]{1,0:T(8,128)(2,1)}) %all-gather.10.cloned.1.call-update) | async-done | bytes 12582928 | tf_op jit(solution)/shard_map/all_gather | solution.py:147
  542.4 176.4 %all-gather.8.cloned.1.call-done = bf16[4096,1536]{1,0:T(8,128)(2,1)} async-done(((bf16[512,1536]{1,0:T(8,128)(2,1)}), bf16[4096,1536]{1,0:T(8,128)(2,1)}) %all-gather.8.cloned.1.call-update) | async-done | bytes 12582928 | tf_op jit(solution)/shard_map/all_gather | solution.py:140
  718.8 14.9 %convolution_convert_fusion = bf16[192,4096]{1,0:T(8,128)(2,1)} fusion(bf16[1536,4096]{1,0:T(8,128)(2,1)} %all-gather.10.cloned.1.call-done, bf16[4096,1536]{1,0:T(8,128)(2,1)} %all-gather.8.cloned.1.call-done, f32[192,1536]{1,0:T(8,128)} %fusion.55, f32[4096]{0:T(1024)S(1)} %copy-done.9, f32[192]{0:T(256)S(1)} %add_rsqrt_fusion.4, ...), kind=kOutput, calls=%fused_computation.7 | convolution fusion | flops 4839112704 | bytes 31081216 | tf_op jit(solution)/shard_map/dot_general | solution.py:145
  733.7 26.4 %reduce-scatter.2.cloned.1.call-done = bf16[48,4096]{1,0:T(8,128)(2,1)} async-done(((bf16[192,4096]{1,0:T(8,128)(2,1)}), bf16[48,4096]{1,0:T(8,128)(2,1)}) %reduce-scatter.2.cloned.1.call-update) | async-done | bytes 393232 | tf_op jit(solution)/shard_map/reduce_scatter | solution.py:150
  760.1 2.1 add_convert_fusion
  (48 shorter events, 0.6 us)
Async XLA Ops:
  6.5 37.6 %copy-start.4 = (bf16[192,512]{1,0:T(8,128)(2,1)S(1)}, bf16[192,512]{1,0:T(8,128)(2,1)}, u32[]{:S(2)}) copy-start(bf16[192,512]{1,0:T(8,128)(2,1)} %param.18) | copy-start | bytes 589828
  6.5 181.2 %all-gather.12.cloned.1.call-start = ((), (), s32[]{:S(2)}) async-start(), calls=%async_computation.5 | async-start | bytes 7864320 | tf_op jit(solution)/shard_map/all_gather | solution.py:14
  44.9 5.3 copy-start.5
  45.0 5.5 copy-start.8
  50.0 0.9 copy-start.6
  84.7 3.1 copy-start.7
  120.3 3.8 copy-start
  130.7 5.7 copy-start.1
  136.5 2.2 copy-start.2
  140.9 225.2 %all-gather.6.cloned.1.call-start = ((), (), s32[]{:S(2)}) async-start(), calls=%async_computation.1 | async-start | bytes 14155776 | tf_op jit(solution)/shard_map/all_gather | solution.py:139
  141.6 400.8 %all-gather.10.cloned.1.call-start = ((), (), s32[]{:S(2)}) async-start(), calls=%async_computation.3 | async-start | bytes 14155776 | tf_op jit(solution)/shard_map/all_gather | solution.py:147
  142.4 576.4 %all-gather.8.cloned.1.call-start = ((), (), s32[]{:S(2)}) async-start(), calls=%async_computation.2 | async-start | bytes 14155776 | tf_op jit(solution)/shard_map/all_gather | solution.py:140
  142.9 617.2 %reduce-scatter.2.cloned.1.call-start = ((), (), s32[]{:S(2)}) async-start(), calls=%async_computation.4 | async-start | bytes 1966080 | tf_op jit(solution)/shard_map/reduce_scatter | solution.py:150
  187.7 4.2 copy-start.3
  192.0 174.1 %copy-start.9 = (f32[4096]{0:T(1024)S(1)}, f32[4096]{0:T(1024)}, u32[]{:S(2)}) copy-start(f32[4096]{0:T(1024)} %param.26) | copy-start | bytes 49156
Sparse Core Ops, SparseCore 0:
  141.0 46.6 all-gather.11
  189.9 176.0 all-gather.5
  368.1 174.2 all-gather.9
  544.5 174.2 all-gather.7
  733.8 26.2 reduce-scatter.1
